TPU v7x, 32 devices: a whole 2x2x4 slice. The times are simulated.
32 devices in a mesh: grp: 2 (over x), ep: 4 (over y, core), tp: 4 (over z).
Axes of the slice: x: 2, y: 2, z: 4, core: 2. Of those that a mesh axis runs over, the one named last changes fastest.
Arguments:
- pool_input: bfloat16 [8192, 1024], P(('grp', 'ep'), 'tp'), parts along dimension 0, may hold values from -6 to 6
- pool_map: bfloat16 [8, 128, 128], replicated, may hold values from -0.5 to 0.5
- pool_scale: float32 [1024], replicated, may hold values from 0.1 to 1.9
- out_weight: bfloat16 [1024, 2048], P(None, 'tp'), may hold values from -0.1875 to 0.1875
- expert_input: bfloat16 [4096, 2048], P(('grp', 'ep', 'tp')), parts along dimension 0, may hold values from -6 to 6
- norm_gain: float32 [2048], replicated, may hold values from 0.1 to 1.9
- routes: int32 [4096, 2], P(('grp', 'ep', 'tp')), parts along dimension 0, may hold values from 0 to 15, all different within a row; in each aligned block of 128 rows (0 to 127, 128 to 255, ...) at most 32 rows name the same one
- route_weight: float32 [4096, 2], P(('grp', 'ep', 'tp')), parts along dimension 0, may hold values from 0.2 to 1.5
- gate_weight: bfloat16 [16, 2048, 512], P(('ep', 'tp')), may hold values from -0.125 to 0.125
- up_weight: bfloat16 [16, 2048, 512], P(('ep', 'tp')), may hold values from -0.125 to 0.125
- down_weight: bfloat16 [16, 512, 2048], P(('ep', 'tp')), may hold values from -0.25 to 0.25
Outputs:
- pool_output: bfloat16 [8192, 2048], P(('grp', 'ep'), 'tp'), parts along dimension 0
- expert_output: bfloat16 [4096, 2048], P(('grp', 'ep', 'tp')), parts along dimension 0
There are 2 independent parts, one for each index of `grp`. A program takes and returns all parts, laid end to end along the dimension named above; an argument that names none is the same for every part. Nothing has to cross between parts.
Inputs may be any that keep to these rules, and one draw needn't show every extreme that they name: `routes`: each row names 2 different experts. In the rows of one device no expert is named more than 32 times, and in every draw some device names some expert exactly 32 times.
All inputs are finite; a program needn't handle non-finite values.
Results may differ from a plain program's by a relative error of at most 0.007.
Values may be sent and summed in bfloat16 or wider, within the bound.
No kernel may reach another device: no remote copies, remote signals or barrier semaphores. Data moves between devices by JAX's collectives and lax.ppermute only.
A program may use at most 64 MiB of HBM per device.

v0:
```python
import jax
import jax.numpy as jnp
from jax import lax
from jax.sharding import PartitionSpec as P

epsilon = 1e-06
halo_depth = 16


def shifted_2(shard, axis, by):
    size = lax.axis_size(axis)
    pairs = [(i, i + by) for i in range(size) if 0 <= i + by < size]
    return lax.ppermute(shard, axis, pairs)


def expert_rows(received, gate_weight, up_weight, down_weight):
    shape_in = received.shape
    flat_rows = received.reshape(-1, shape_in[-1])
    gate_part = jnp.dot(flat_rows, gate_weight[0], preferred_element_type=jnp.float32)
    up_part = jnp.dot(flat_rows, up_weight[0], preferred_element_type=jnp.float32)
    hidden = (jax.nn.silu(gate_part) * up_part).astype(jnp.bfloat16)
    result = jnp.dot(hidden, down_weight[0], preferred_element_type=jnp.float32).astype(
        jnp.bfloat16
    )
    return result.reshape(shape_in)


def pool_half(pool_input, pool_map, pool_scale, out_weight):
    row_count, width_local = pool_input.shape
    group_dim = pool_map.shape[1]
    groups_local = width_local // group_dim
    last_rows = pool_input[row_count - halo_depth :]
    earlier_rows = shifted_2(last_rows, "ep", 1)
    extended = jnp.concatenate([earlier_rows, pool_input], axis=0).astype(jnp.float32)
    first_group = lax.axis_index("tp") * groups_local
    group_ids = first_group + jnp.arange(width_local, dtype=jnp.int32) // group_dim
    window = jnp.left_shift(jnp.int32(2), group_ids % 4)
    summed = jnp.zeros((row_count, width_local), jnp.float32)
    for offset in range(halo_depth):
        shifted = extended[halo_depth - offset : halo_depth - offset + row_count]
        summed = summed + jnp.where(offset < window, shifted, 0.0)
    positions = lax.axis_index("ep") * row_count + jnp.arange(row_count, dtype=jnp.int32)
    counted = jnp.minimum(positions[:, None] + 1, window[None, :]).astype(jnp.float32)
    pooled = (summed / counted - extended[halo_depth:]).astype(jnp.bfloat16)
    maps_local = lax.dynamic_slice_in_dim(pool_map, first_group, groups_local, 0)
    scales_local = lax.dynamic_slice_in_dim(pool_scale, first_group * group_dim, width_local, 0)
    mapped = jnp.einsum(
        "rgc,gcd->rgd",
        pooled.reshape(row_count, groups_local, group_dim),
        maps_local,
        preferred_element_type=jnp.float32,
    )
    mapped = (mapped.reshape(row_count, width_local) * scales_local).astype(jnp.bfloat16)
    projected = jnp.dot(
        lax.all_gather(mapped, "tp", axis=1, tiled=True),
        out_weight,
        preferred_element_type=jnp.float32,
    )
    return projected.astype(jnp.bfloat16)


def expert_half(expert_input, norm_gain, routes, route_weight, gate_weight, up_weight, down_weight):
    row_count, model_width = expert_input.shape
    top_count = routes.shape[1]
    widened = expert_input.astype(jnp.float32)
    normed = (
        widened
        * lax.rsqrt(jnp.mean(widened * widened, axis=1, keepdims=True) + epsilon)
        * norm_gain
    )
    normed = normed.astype(jnp.bfloat16)
    ep_count = lax.axis_size("ep")
    tp_count = lax.axis_size("tp")
    experts = ep_count * tp_count
    capacity = 2 * row_count * top_count // experts
    copies = row_count * top_count
    flat_routes = routes.reshape(copies)
    onehot = (flat_routes[:, None] == jnp.arange(experts, dtype=jnp.int32)[None, :]).astype(
        jnp.int32
    )
    slot_index = jnp.sum((jnp.cumsum(onehot, axis=0) - onehot) * onehot, axis=1)
    target = flat_routes * capacity + slot_index
    source_row = jnp.arange(copies, dtype=jnp.int32) // top_count
    slot_table = jnp.full((experts * capacity,), row_count, jnp.int32).at[target].set(source_row)
    padded = jnp.concatenate([normed, jnp.zeros((1, model_width), jnp.bfloat16)], axis=0)
    outgoing = padded[slot_table].reshape(experts, capacity, model_width)
    results = expert_rows(
        lax.all_to_all(outgoing, ("ep", "tp"), split_axis=0, concat_axis=0, tiled=True),
        gate_weight,
        up_weight,
        down_weight,
    )
    returned = lax.all_to_all(results, ("ep", "tp"), split_axis=0, concat_axis=0, tiled=True)
    returned = returned.reshape(experts * capacity, model_width)
    picked = returned[target].astype(jnp.float32) * route_weight.reshape(copies)[:, None]
    return picked.reshape(row_count, top_count, model_width).sum(axis=1).astype(jnp.bfloat16)


def on_device(
    pool_input,
    pool_map,
    pool_scale,
    out_weight,
    expert_input,
    norm_gain,
    routes,
    route_weight,
    gate_weight,
    up_weight,
    down_weight,
):
    pool_output = pool_half(pool_input, pool_map, pool_scale, out_weight)
    expert_output = expert_half(
        expert_input, norm_gain, routes, route_weight, gate_weight, up_weight, down_weight
    )
    return (pool_output, expert_output)


def solution(mesh):
    return jax.shard_map(
        on_device,
        mesh=mesh,
        in_specs=(
            P(("grp", "ep"), "tp"),
            P(),
            P(),
            P(None, "tp"),
            P(("grp", "ep", "tp"), None),
            P(),
            P(("grp", "ep", "tp"), None),
            P(("grp", "ep", "tp"), None),
            P(("ep", "tp"), None, None),
            P(("ep", "tp"), None, None),
            P(("ep", "tp"), None, None),
        ),
        out_specs=(P(("grp", "ep"), "tp"), P(("grp", "ep", "tp"), None)),
        check_vma=False,
    )
```

profile of v0, /device:TPU:0, one launch (start us, length us, event | category | flops | bytes accessed | tf_op | source)
XLA Modules:
  0.0 192.7 jit_solution(14643236694304669269)
XLA Ops:
  7.2 0.9 copy.19
  8.4 0.7 broadcast_multiply_fusion
  9.1 0.6 reduce-window.6
  10.3 1.4 scatter_custom_fusion
  11.7 1.2 fusion.11
  12.9 1.2 fusion.13
  14.2 3.3 %gather_fusion = bf16[512,2048]{1,0:T(8,128)(2,1)} fusion(bf16[129,2048]{1,0:T(8,128)(2,1)S(1)} %concatenate.7, s32[1024]{0:T(1024)S(1)} %pad_clamp_fusion.1), kind=kCustom, calls=%fused_computation | custom fusion | bytes 4196352 | tf_op jit(solution)/shard_map/gather | solution.py:86
  17.6 7.5 %all-to-all-start = ((bf16[16,32,2048]{2,1,0:T(8,128)(2,1)}), bf16[16,32,2048]{2,1,0:T(8,128)(2,1)}, u32[]{:S(2)}, u32[]{:S(2)}) async-start(bf16[16,32,2048]{2,1,0:T(8,128)(2,1)} %bitcast.57), calls=%async_computation | async-start | bytes 4194304 | tf_op jit(solution)/shard_map/all_to_all | solution.py:88
  25.0 0.7 slice.58
  25.8 2.2 %collective-permute-start = (bf16[16,256]{1,0:T(8,128)(2,1)S(1)}, bf16[16,256]{1,0:T(8,128)(2,1)S(1)}, u32[]{:S(2)}, u32[]{:S(2)}) collective-permute-start(bf16[16,256]{1,0:T(8,128)(2,1)S(1)} %slice.58), channel_id=1, source_target_pairs={{0,4},{4,8},{8,12},{1,5},{5,9},{9,13},{2,6},{6,10},{10,14},{3,7},{... | collective-permute-start | bytes 24584 | tf_op jit(solution)/shard_map/ppermute | solution.py:13
  28.2 0.8 dynamic_slice.7
  29.0 1.1 maximum_convert_fusion
  30.1 44.3 %all-to-all-done = bf16[16,32,2048]{2,1,0:T(8,128)(2,1)} async-done(((bf16[16,32,2048]{2,1,0:T(8,128)(2,1)}), bf16[16,32,2048]{2,1,0:T(8,128)(2,1)}, u32[]{:S(2)}, u32[]{:S(2)}) %all-to-all-start) | async-done | bytes 2097184 | tf_op jit(solution)/shard_map/all_to_all | solution.py:88
  74.4 4.4 %fusion.3 = f32[512,512]{1,0:T(8,128)} fusion(bf16[512,2048]{1,0:T(8,128)(2,1)} %bitcast.6, bf16[1,2048,512]{2,1,0:T(8,128)(2,1)} %param.19), kind=kOutput, calls=%fused_computation.7 | convolution fusion | flops 1073741824 | bytes 5242880 | tf_op jit(solution)/shard_map/dot_general | solution.py:19
  78.9 6.3 %convolution_convert_fusion = bf16[512,2048]{1,0:T(8,128)(2,1)} fusion(bf16[1,512,2048]{2,1,0:T(8,128)(2,1)S(1)} %copy-done, bf16[512,2048]{1,0:T(8,128)(2,1)} %bitcast.6, bf16[1,2048,512]{2,1,0:T(8,128)(2,1)} %param.20, f32[512,512]{1,0:T(8,128)} %fusion.3), kind=kOutput, calls=%fused_computation.3 | convolution fusion | flops 2150105088 | bytes 9437184 | tf_op jit(solution)/shard_map/dot_general | solution.py:22
  85.1 4.4 %all-to-all-start.1 = ((bf16[16,32,2048]{2,1,0:T(8,128)(2,1)}), bf16[16,32,2048]{2,1,0:T(8,128)(2,1)}, u32[]{:S(2)}, u32[]{:S(2)}) async-start(bf16[16,32,2048]{2,1,0:T(8,128)(2,1)} %bitcast.58), calls=%async_computation.1 | async-start | bytes 4194304 | tf_op jit(solution)/shard_map/all_to_all | solution.py:93
  89.6 0.2 all-gather.2.cloned.1.call-start
  89.8 3.8 %fusion.35 = f32[2,128,1024]{2,1,0:T(8,128)S(1)} fusion(bf16[8,128,128]{2,1,0:T(8,128)(2,1)} %param.12, s32[]{:T(128)S(6)} %select_n.92, s32[256]{0:T(256)S(1)} %fusion.46, s32[1024]{0:T(1024)S(1)} %add_add_fusion, f32[1040,256]{1,0:T(8,128)S(1)} %maximum_convert_fusion, pred[256]{0:T(512)(128)(4,1)S(1)} %get-tuple-element.2, ...), kind=kOutput, calls=%fused_computation.54 | convolution fusion | flops 76546048 | bytes 17904644 | tf_op jit(solution)/shard_map/rgc,gcd->rgd/dot_general | solution.py:47
  93.7 0.9 fusion.31
  94.8 75.0 %all-gather.2.cloned.1.call-done = bf16[1024,1024]{0,1:T(8,128)(2,1)} async-done(((bf16[1024,256]{0,1:T(8,128)(2,1)}), bf16[1024,1024]{0,1:T(8,128)(2,1)}) %all-gather.2.cloned.1.call-update) | async-done | bytes 2097168 | tf_op jit(solution)/shard_map/all_gather | solution.py:55
  169.8 3.9 %convolution_convert_fusion.1 = bf16[1024,512]{1,0:T(8,128)(2,1)} fusion(bf16[1024,1024]{0,1:T(8,128)(2,1)} %all-gather.2.cloned.1.call-done, bf16[1024,512]{1,0:T(8,128)(2,1)S(1)} %copy-done.2), kind=kOutput, calls=%fused_computation.10 | convolution fusion | flops 1074266112 | bytes 4194304 | tf_op jit(solution)/shard_map/dot_general | solution.py:54
  173.6 4.2 %gather_fusion.1 = bf16[256,2048]{1,0:T(8,128)(2,1)S(1)} fusion(bf16[512,2048]{1,0:T(8,128)(2,1)} %bitcast.11, s32[1024]{0:T(1024)S(1)} %pad_clamp_fusion), kind=kCustom, calls=%fused_computation.1 | custom fusion | bytes 2098176 | tf_op jit(solution)/shard_map/gather | solution.py:95
  177.9 2.4 %reshape.127 = f32[128,2,2048]{2,1,0:T(2,128)} reshape(bf16[256,2048]{1,0:T(8,128)(2,1)S(1)} %gather_fusion.1) | data formatting | bytes 3145728 | tf_op jit(solution)/shard_map/convert_element_type | solution.py:95
  180.2 5.6 %multiply_reduce_fusion = bf16[128,2048]{1,0:T(8,128)(2,1)} fusion(f32[128,2,2048]{2,1,0:T(2,128)} %reshape.127, f32[128,2]{1,0:T(8,128)S(1)} %copy.22), kind=kLoop, calls=%fused_computation.9 | loop fusion | flops 786432 | bytes 2622464 | tf_op jit(solution)/shard_map/reduce_sum | solution.py:96
  (36 shorter events, 1.2 us)
Async XLA Ops:
  7.2 71.7 %copy-start = (bf16[1,512,2048]{2,1,0:T(8,128)(2,1)S(1)}, bf16[1,512,2048]{2,1,0:T(8,128)(2,1)}, u32[]{:S(2)}) copy-start(bf16[1,512,2048]{2,1,0:T(8,128)(2,1)} %param.21) | copy-start | bytes 6291460
  17.6 56.8 %all-to-all-start = ((bf16[16,32,2048]{2,1,0:T(8,128)(2,1)}), bf16[16,32,2048]{2,1,0:T(8,128)(2,1)}, u32[]{:S(2)}, u32[]{:S(2)}) async-start(bf16[16,32,2048]{2,1,0:T(8,128)(2,1)} %bitcast.57), calls=%async_computation | async-start | bytes 4194304 | tf_op jit(solution)/shard_map/all_to_all | solution.py:88
  25.8 3.2 %collective-permute-start = (bf16[16,256]{1,0:T(8,128)(2,1)S(1)}, bf16[16,256]{1,0:T(8,128)(2,1)S(1)}, u32[]{:S(2)}, u32[]{:S(2)}) collective-permute-start(bf16[16,256]{1,0:T(8,128)(2,1)S(1)} %slice.58), channel_id=1, source_target_pairs={{0,4},{4,8},{8,12},{1,5},{5,9},{9,13},{2,6},{6,10},{10,14},{3,7},{... | collective-permute-start | bytes 24584 | tf_op jit(solution)/shard_map/ppermute | solution.py:13
  85.1 88.5 %all-to-all-start.1 = ((bf16[16,32,2048]{2,1,0:T(8,128)(2,1)}), bf16[16,32,2048]{2,1,0:T(8,128)(2,1)}, u32[]{:S(2)}, u32[]{:S(2)}) async-start(bf16[16,32,2048]{2,1,0:T(8,128)(2,1)} %bitcast.58), calls=%async_computation.1 | async-start | bytes 4194304 | tf_op jit(solution)/shard_map/all_to_all | solution.py:93
  89.6 80.2 %all-gather.2.cloned.1.call-start = ((), (), s32[]{:S(2)}) async-start(), calls=%async_computation.2 | async-start | bytes 2621440 | tf_op jit(solution)/shard_map/all_gather | solution.py:55
  93.7 1.0 copy-start.1
  93.7 76.1 %copy-start.2 = (bf16[1024,512]{1,0:T(8,128)(2,1)S(1)}, bf16[1024,512]{1,0:T(8,128)(2,1)}, u32[]{:S(2)}) copy-start(bf16[1024,512]{1,0:T(8,128)(2,1)} %param.14) | copy-start | bytes 3145732
Sparse Core Ops, SparseCore 0:
  94.7 74.9 all-gather.1
where the time goes:
time: 193 us
  waiting for transfers between devices  119 us (62%)
  matrix products  18.4 us (10%)
  local copies, waits for them, and re-layouts  14.6 us (8%)
  starting transfers between devices  14.4 us (7%)
  between operations  14.2 us (7%)
  other arithmetic  11.7 us (6%)
    all_gather x1, waiting for transfers between devices, pool_half(): lax.all_gather(mapped, 'tp', axis=1, tiled=True)  75 us
    all_to_all x1, waiting for transfers between devices, expert_half(): lax.all_to_all(outgoing, ('ep', 'tp'), split_axis=0, concat_axis=0, tiled...  44.3 us
    all_to_all x1, starting transfers between devices, expert_half(): lax.all_to_all(outgoing, ('ep', 'tp'), split_axis=0, concat_axis=0, tiled...  7.46 us
    dot_general x1, matrix products, expert_rows(): jnp.dot(hidden, down_weight[0], preferred_element_type=jnp.float32)  6.28 us
    reduce_sum x1, other arithmetic, expert_half(): picked.reshape(row_count, top_count, model_width).sum(axis=1)  5.59 us
    dot_general x1, matrix products, expert_rows(): jnp.dot(flat_rows, gate_weight[0], preferred_element_type=jnp.float32)  4.44 us
    all_to_all x1, starting transfers between devices, expert_half(): lax.all_to_all(results, ('ep', 'tp'), split_axis=0, concat_axis=0, tiled=...  4.44 us
    gather x1, local copies, waits for them, and re-layouts, expert_half(): returned[target].astype(jnp.float32) * route_weight.reshape(copies)[:, None]  4.22 us
  transfers between devices with their start and end apart: 4, of which 2 were waited for; matrix products, arithmetic and copies ran while one was open for 6% of the time, Pallas kernels for 0%

commit v1 on v0

--- a/solution.py
+++ b/solution.py
@@ -52,7 +52,7 @@
     )
     mapped = (mapped.reshape(row_count, width_local) * scales_local).astype(jnp.bfloat16)
     projected = jnp.dot(
-        lax.all_gather(mapped, "tp", axis=1, tiled=True),
+        jnp.concatenate(lax.all_gather(mapped, "tp"), axis=1),
         out_weight,
         preferred_element_type=jnp.float32,
     )

time: 193 us -> 198 us (1.026)
  local copies, waits for them, and re-layouts: 14.6 us -> 20.2 us
  waiting for transfers between devices: 119 us -> 117 us
    all_gather x0 -> x1, local copies, waits for them, and re-layouts: none -> 3.98 us  [pool_half(): lax.all_gather(mapped, 'tp')]
    all_gather x1, waiting for transfers between devices: 75 us -> 73 us  [pool_half(): lax.all_gather(mapped, 'tp')]
  transfers between devices with their start and end apart: 4 -> 4, of which waited for: 2 -> 2; matrix products, arithmetic and copies ran while one was open for 6% -> 9% of each run, Pallas kernels for 0% -> 0%
where the time goes in v1:
time: 198 us
  waiting for transfers between devices  117 us (59%)
  local copies, waits for them, and re-layouts  20.2 us (10%)
  matrix products  19.8 us (10%)
  starting transfers between devices  14.4 us (7%)
  between operations  14.2 us (7%)
  other arithmetic  11.6 us (6%)
    all_gather x1, waiting for transfers between devices, pool_half(): lax.all_gather(mapped, 'tp')  73 us
    all_to_all x1, waiting for transfers between devices, expert_half(): lax.all_to_all(outgoing, ('ep', 'tp'), split_axis=0, concat_axis=0, tiled...  44.3 us
    all_to_all x1, starting transfers between devices, expert_half(): lax.all_to_all(outgoing, ('ep', 'tp'), split_axis=0, concat_axis=0, tiled...  7.46 us
    dot_general x1, matrix products, expert_rows(): jnp.dot(hidden, down_weight[0], preferred_element_type=jnp.float32)  6.28 us
    reduce_sum x1, other arithmetic, expert_half(): picked.reshape(row_count, top_count, model_width).sum(axis=1)  5.59 us
    dot_general x1, matrix products, pool_half(): jnp.einsum('rgc,gcd->rgd', pooled.reshape(row_count, groups_local, group_...  5.25 us
    dot_general x1, matrix products, expert_rows(): jnp.dot(flat_rows, gate_weight[0], preferred_element_type=jnp.float32)  4.44 us
    all_to_all x1, starting transfers between devices, expert_half(): lax.all_to_all(results, ('ep', 'tp'), split_axis=0, concat_axis=0, tiled=...  4.44 us
  transfers between devices with their start and end apart: 4, of which 2 were waited for; matrix products, arithmetic and copies ran while one was open for 9% of the time, Pallas kernels for 0%

profile of v1, /device:TPU:0, one launch (start us, length us, event | category | flops | bytes accessed | tf_op | source)
XLA Modules:
  0.0 197.5 jit_solution(8453248180965165333)
XLA Ops:
  7.2 0.9 copy.36
  8.4 0.7 broadcast_multiply_fusion
  10.3 1.4 scatter_custom_fusion
  11.7 1.2 fusion.11
  12.9 1.2 fusion.13
  14.2 3.3 %gather_fusion = bf16[512,2048]{1,0:T(8,128)(2,1)} fusion(bf16[129,2048]{1,0:T(8,128)(2,1)S(1)} %concatenate.7, s32[1024]{0:T(1024)S(1)} %pad_clamp_fusion.1), kind=kCustom, calls=%fused_computation | custom fusion | bytes 4196352 | tf_op jit(solution)/shard_map/gather | solution.py:86
  17.6 7.5 %all-to-all-start = ((bf16[16,32,2048]{2,1,0:T(8,128)(2,1)}), bf16[16,32,2048]{2,1,0:T(8,128)(2,1)}, u32[]{:S(2)}, u32[]{:S(2)}) async-start(bf16[16,32,2048]{2,1,0:T(8,128)(2,1)} %bitcast.57), calls=%async_computation | async-start | bytes 4194304 | tf_op jit(solution)/shard_map/all_to_all | solution.py:88
  25.0 0.7 slice.58
  25.8 2.2 %collective-permute-start = (bf16[16,256]{1,0:T(8,128)(2,1)S(1)}, bf16[16,256]{1,0:T(8,128)(2,1)S(1)}, u32[]{:S(2)}, u32[]{:S(2)}) collective-permute-start(bf16[16,256]{1,0:T(8,128)(2,1)S(1)} %slice.58), channel_id=1, source_target_pairs={{0,4},{4,8},{8,12},{1,5},{5,9},{9,13},{2,6},{6,10},{10,14},{3,7},{... | collective-permute-start | bytes 24584 | tf_op jit(solution)/shard_map/ppermute | solution.py:13
  28.2 0.8 dynamic_slice.7
  29.0 1.1 maximum_convert_fusion
  30.1 44.3 %all-to-all-done = bf16[16,32,2048]{2,1,0:T(8,128)(2,1)} async-done(((bf16[16,32,2048]{2,1,0:T(8,128)(2,1)}), bf16[16,32,2048]{2,1,0:T(8,128)(2,1)}, u32[]{:S(2)}, u32[]{:S(2)}) %all-to-all-start) | async-done | bytes 2097184 | tf_op jit(solution)/shard_map/all_to_all | solution.py:88
  74.4 4.4 %fusion.3 = f32[512,512]{1,0:T(8,128)} fusion(bf16[512,2048]{1,0:T(8,128)(2,1)} %bitcast.8, bf16[1,2048,512]{2,1,0:T(8,128)(2,1)} %param.19), kind=kOutput, calls=%fused_computation.7 | convolution fusion | flops 1073741824 | bytes 5242880 | tf_op jit(solution)/shard_map/dot_general | solution.py:19
  78.9 6.3 %convolution_convert_fusion = bf16[512,2048]{1,0:T(8,128)(2,1)} fusion(bf16[1,512,2048]{2,1,0:T(8,128)(2,1)S(1)} %copy-done, bf16[512,2048]{1,0:T(8,128)(2,1)} %bitcast.8, bf16[1,2048,512]{2,1,0:T(8,128)(2,1)} %param.20, f32[512,512]{1,0:T(8,128)} %fusion.3), kind=kOutput, calls=%fused_computation.3 | convolution fusion | flops 2150105088 | bytes 9437184 | tf_op jit(solution)/shard_map/dot_general | solution.py:22
  85.1 4.4 %all-to-all-start.1 = ((bf16[16,32,2048]{2,1,0:T(8,128)(2,1)}), bf16[16,32,2048]{2,1,0:T(8,128)(2,1)}, u32[]{:S(2)}, u32[]{:S(2)}) async-start(bf16[16,32,2048]{2,1,0:T(8,128)(2,1)} %bitcast.58), calls=%async_computation.1 | async-start | bytes 4194304 | tf_op jit(solution)/shard_map/all_to_all | solution.py:93
  89.8 5.3 %fusion.34 = f32[2,128,1024]{2,1,0:T(8,128)} fusion(bf16[8,128,128]{2,1,0:T(8,128)(2,1)} %param.12, s32[]{:T(128)S(6)} %select_n.92, s32[256]{0:T(256)S(1)} %fusion.45, s32[1024]{0:T(1024)S(1)} %add_add_fusion, f32[1040,256]{1,0:T(8,128)S(1)} %maximum_convert_fusion, pred[256]{0:T(512)(128)(4,1)S(1)} %get-tuple-element.2, ...), kind=kOutput, calls=%fused_computation.53 | convolution fusion | flops 76546048 | bytes 17904644 | tf_op jit(solution)/shard_map/rgc,gcd->rgd/dot_general | solution.py:47
  95.1 1.6 copy.33
  96.6 0.9 multiply_convert_fusion
  97.7 73.0 %all-gather.2.cloned.1.call-done = bf16[4,1024,256]{2,1,0:T(8,128)(2,1)} async-done(((bf16[1,1024,256]{2,1,0:T(8,128)(2,1)}), bf16[4,1024,256]{2,1,0:T(8,128)(2,1)}) %all-gather.2.cloned.1.call-update) | async-done | bytes 2097168 | tf_op jit(solution)/shard_map/all_gather | solution.py:55
  170.7 4.0 %copy.34 = bf16[4,1024,256]{1,2,0:T(8,128)(2,1)} copy(bf16[4,1024,256]{2,1,0:T(8,128)(2,1)} %all-gather.2.cloned.1.call-done) | data formatting | bytes 4194304 | tf_op jit(solution)/shard_map/all_gather | solution.py:55
  174.6 3.9 %convolution_convert_fusion.1 = bf16[1024,512]{1,0:T(8,128)(2,1)} fusion(bf16[1024,1024]{0,1:T(8,128)(2,1)} %bitcast.59, bf16[1024,512]{1,0:T(8,128)(2,1)S(1)} %copy-done.2), kind=kOutput, calls=%fused_computation.10 | convolution fusion | flops 1074266112 | bytes 4194304 | tf_op jit(solution)/shard_map/dot_general | solution.py:54
  178.5 4.2 %gather_fusion.1 = bf16[256,2048]{1,0:T(8,128)(2,1)S(1)} fusion(bf16[512,2048]{1,0:T(8,128)(2,1)} %bitcast.13, s32[1024]{0:T(1024)S(1)} %pad_clamp_fusion), kind=kCustom, calls=%fused_computation.1 | custom fusion | bytes 2098176 | tf_op jit(solution)/shard_map/gather | solution.py:95
  182.7 2.4 %reshape.169 = f32[128,2,2048]{2,1,0:T(2,128)} reshape(bf16[256,2048]{1,0:T(8,128)(2,1)S(1)} %gather_fusion.1) | data formatting | bytes 3145728 | tf_op jit(solution)/shard_map/convert_element_type | solution.py:95
  185.1 5.6 %multiply_reduce_fusion = bf16[128,2048]{1,0:T(8,128)(2,1)} fusion(f32[128,2,2048]{2,1,0:T(2,128)} %reshape.169, f32[128,2]{1,0:T(8,128)S(1)} %copy.39), kind=kLoop, calls=%fused_computation.9 | loop fusion | flops 786432 | bytes 2622464 | tf_op jit(solution)/shard_map/reduce_sum | solution.py:96
  (38 shorter events, 2.0 us)
Async XLA Ops:
  7.2 71.7 %copy-start = (bf16[1,512,2048]{2,1,0:T(8,128)(2,1)S(1)}, bf16[1,512,2048]{2,1,0:T(8,128)(2,1)}, u32[]{:S(2)}) copy-start(bf16[1,512,2048]{2,1,0:T(8,128)(2,1)} %param.21) | copy-start | bytes 6291460
  17.6 56.8 %all-to-all-start = ((bf16[16,32,2048]{2,1,0:T(8,128)(2,1)}), bf16[16,32,2048]{2,1,0:T(8,128)(2,1)}, u32[]{:S(2)}, u32[]{:S(2)}) async-start(bf16[16,32,2048]{2,1,0:T(8,128)(2,1)} %bitcast.57), calls=%async_computation | async-start | bytes 4194304 | tf_op jit(solution)/shard_map/all_to_all | solution.py:88
  25.8 3.2 %collective-permute-start = (bf16[16,256]{1,0:T(8,128)(2,1)S(1)}, bf16[16,256]{1,0:T(8,128)(2,1)S(1)}, u32[]{:S(2)}, u32[]{:S(2)}) collective-permute-start(bf16[16,256]{1,0:T(8,128)(2,1)S(1)} %slice.58), channel_id=1, source_target_pairs={{0,4},{4,8},{8,12},{1,5},{5,9},{9,13},{2,6},{6,10},{10,14},{3,7},{... | collective-permute-start | bytes 24584 | tf_op jit(solution)/shard_map/ppermute | solution.py:13
  85.1 93.4 %all-to-all-start.1 = ((bf16[16,32,2048]{2,1,0:T(8,128)(2,1)}), bf16[16,32,2048]{2,1,0:T(8,128)(2,1)}, u32[]{:S(2)}, u32[]{:S(2)}) async-start(bf16[16,32,2048]{2,1,0:T(8,128)(2,1)} %bitcast.58), calls=%async_computation.1 | async-start | bytes 4194304 | tf_op jit(solution)/shard_map/all_to_all | solution.py:93
  89.6 81.1 %all-gather.2.cloned.1.call-start = ((), (), s32[]{:S(2)}) async-start(), calls=%async_computation.2 | async-start | bytes 2621440 | tf_op jit(solution)/shard_map/all_gather | solution.py:55
  95.1 2.5 %copy-start.1 = (f32[128,2]{0,1:T(2,128)S(1)}, f32[128,2]{0,1:T(2,128)}, u32[]{:S(2)}) copy-start(f32[128,2]{0,1:T(2,128)} %param.18) | copy-start | bytes 3076
  97.7 77.0 %copy-start.2 = (bf16[1024,512]{1,0:T(8,128)(2,1)S(1)}, bf16[1024,512]{1,0:T(8,128)(2,1)}, u32[]{:S(2)}) copy-start(bf16[1024,512]{1,0:T(8,128)(2,1)} %param.14) | copy-start | bytes 3145732
Sparse Core Ops, SparseCore 0:
  97.7 72.9 all-gather.1
